TPU v7x, 32 devices: a whole 2x2x4 slice. The times are simulated.
32 devices in a mesh: ep: 8 (over z, core), tp: 4 (over y, x).
Axes of the slice: x: 2, y: 2, z: 4, core: 2. Of those that a mesh axis runs over, the one named last changes fastest.
Arguments:
- queries: bfloat16 [2048, 2048], P('ep', 'tp'), may hold values from -6 to 6
- keys: bfloat16 [2048, 2048], P('ep', 'tp'), may hold values from -6 to 6
- values: bfloat16 [2048, 2048], P('ep', 'tp'), may hold values from -6 to 6
- gates: bfloat16 [2048, 2048], P('ep', 'tp'), may hold values from -6 to 6
- log_decay: float32 [2048, 16], P('ep', 'tp'), may hold values from -2 to 0
- out_weight: bfloat16 [2048, 2048], P(None, 'tp'), may hold values from -0.125 to 0.125
- moe_rows: bfloat16 [2048, 2048], P('ep'), may hold values from -140 to 140
- moe_gain: bfloat16 [2048], replicated, may hold values from 0.099609375 to 1.8984375
- routes: int32 [2048, 2], P('ep'), may hold values from 0 to 7, as said below
- route_weights: float32 [2048, 2], P('ep'), may hold values from 0.1 to 1
- gate_proj: bfloat16 [8, 2048, 4096], P('ep', None, 'tp'), may hold values from -0.125 to 0.125
- up_proj: bfloat16 [8, 2048, 4096], P('ep', None, 'tp'), may hold values from -0.125 to 0.125
- down_proj: bfloat16 [8, 4096, 2048], P('ep', None, 'tp'), may hold values from -0.09375 to 0.09375
Outputs:
- mixer_out: bfloat16 [2048, 2048], P('ep', 'tp')
- moe_out: bfloat16 [2048, 2048], P('ep', 'tp')
Inputs may be any that keep to these rules, and one draw needn't show every extreme that they name: `routes`: each row names two different experts of one group of 8 consecutive experts; in each aligned block of 256 rows every expert is named by exactly 64 rows.
All inputs are finite; a program needn't handle non-finite values.
Results may differ from a plain program's by a relative error of at most 0.011.
Values may be sent and summed in bfloat16 or wider, within the bound.
A program may use at most 64 MiB of HBM per device.

v0:
```python
import jax
import jax.numpy as jnp
from jax import lax
from jax.sharding import PartitionSpec as P

BLOCK = 128


def carried_in(value, axis, join, neutral):
    count, mine = (lax.axis_size(axis), lax.axis_index(axis))
    pieces = jax.tree.map(lambda part: lax.all_gather(part, axis), value)
    total = jax.tree.map(
        lambda part, zero: jnp.full_like(part, 0) + jnp.asarray(zero, part.dtype), value, neutral
    )

    def turn(position, total):
        longer = join(total, jax.tree.map(lambda part: part[position], pieces))
        return jax.tree.map(lambda new, old: jnp.where(position < mine, new, old), longer, total)

    return lax.fori_loop(0, count - 1, turn, total)


def rotate(source, positions, heads_here, factor):
    row_count, feat_width = source.shape
    head_dim = feat_width // heads_here
    half_dim = head_dim // 2
    values_f = source.astype(jnp.float32).reshape(row_count, heads_here, head_dim)
    inverse = 10000.0 ** (-jnp.arange(half_dim, dtype=jnp.float32) / half_dim)
    angles = positions[:, None] * inverse[None, :]
    cosine = jnp.cos(angles)[:, None, :]
    sine_part = jnp.sin(angles)[:, None, :]
    first_half = values_f[..., :half_dim]
    second_half = values_f[..., half_dim:]
    turned = jnp.concatenate(
        [
            first_half * cosine - second_half * sine_part,
            first_half * sine_part + second_half * cosine,
        ],
        axis=-1,
    )
    return (turned * factor).astype(jnp.bfloat16).reshape(row_count, feat_width)


def chain_states(earlier, later):
    return (earlier[0] * later[0], later[0][:, None, None] * earlier[1] + later[1])


def retention_half(queries, keys, values, gates, log_decay, out_weight):
    row_count, feat_width = queries.shape
    heads_here = log_decay.shape[1]
    head_dim = feat_width // heads_here
    block_count = row_count // BLOCK
    positions = (lax.axis_index("ep") * row_count + jnp.arange(row_count, dtype=jnp.int32)).astype(
        jnp.float32
    )
    rot_q = rotate(queries, positions, heads_here, 1.0)
    rot_k = rotate(keys, positions, heads_here, head_dim ** (-0.5))
    block_shape = (block_count, BLOCK, heads_here, head_dim)
    q_blocks = rot_q.reshape(block_shape)
    k_blocks = rot_k.reshape(block_shape)
    v_blocks = values.reshape(block_shape)
    cumulative = jnp.cumsum(log_decay.reshape(block_count, BLOCK, heads_here), axis=1)
    across = jnp.swapaxes(cumulative, 1, 2)
    spread = across[..., :, None] - across[..., None, :]
    causal = jnp.arange(BLOCK)[:, None] >= jnp.arange(BLOCK)[None, :]
    weights = jnp.where(causal, jnp.exp(jnp.where(causal, spread, 0.0)), 0.0)
    scores = jnp.einsum("nihd,njhd->nhij", q_blocks, k_blocks, preferred_element_type=jnp.float32)
    rounded = (scores * weights).astype(jnp.bfloat16)
    inside = jnp.einsum("nhij,njhd->nihd", rounded, v_blocks, preferred_element_type=jnp.float32)
    ending = cumulative[:, -1, :]
    k_scaled = k_blocks.astype(jnp.float32) * jnp.exp(ending[:, None, :] - cumulative)[..., None]
    updates = jnp.einsum(
        "njhd,njhe->nhde", k_scaled, v_blocks.astype(jnp.float32), precision=lax.Precision.HIGHEST
    )

    def advance(carry_state, member):
        return (jnp.exp(member[0])[:, None, None] * carry_state + member[1], carry_state)

    zero_state = jnp.zeros((heads_here, head_dim, head_dim), jnp.float32)
    local_end, before = lax.scan(advance, zero_state, (ending, updates))
    device_decay = jnp.exp(jnp.sum(ending, axis=0))
    incoming = carried_in(
        (device_decay, local_end), "ep", chain_states, (jnp.ones_like(device_decay), zero_state)
    )
    leading = jnp.cumsum(ending, axis=0) - ending
    entering = before + jnp.exp(leading)[:, :, None, None] * incoming[1][None]
    carried = (
        jnp.einsum(
            "nihd,nhde->nihe",
            q_blocks.astype(jnp.float32),
            entering,
            precision=lax.Precision.HIGHEST,
        )
        * jnp.exp(cumulative)[..., None]
    )
    retained = (inside + carried).reshape(row_count, heads_here, head_dim)
    gate_f = gates.astype(jnp.float32).reshape(row_count, heads_here, head_dim)
    scaled = retained * lax.rsqrt(jnp.mean(retained * retained, axis=-1, keepdims=True) + 1e-05)
    head_out = (scaled * jax.nn.silu(gate_f)).astype(jnp.bfloat16).reshape(row_count, feat_width)
    projected = jnp.dot(
        lax.all_gather(head_out, "tp", axis=1, tiled=True),
        out_weight,
        preferred_element_type=jnp.float32,
    )
    return projected.astype(jnp.bfloat16)


def expert_half(moe_rows, moe_gain, routes, route_weights, gate_proj, up_proj, down_proj):
    row_count, feat_width = moe_rows.shape
    experts = lax.axis_size("ep")
    capacity = 2 * row_count // experts
    as_float = moe_rows.astype(jnp.float32)
    normed = (
        as_float
        * lax.rsqrt(jnp.mean(as_float * as_float, axis=-1, keepdims=True) + 1e-06)
        * moe_gain.astype(jnp.float32)
    ).astype(jnp.bfloat16)
    flat_ids = routes.reshape(-1)
    onehot = (flat_ids[:, None] == jnp.arange(experts, dtype=jnp.int32)[None, :]).astype(jnp.int32)
    slot_rank = jnp.sum((jnp.cumsum(onehot, axis=0) - onehot) * onehot, axis=1)
    target = flat_ids * capacity + slot_rank
    source_row = (
        jnp.zeros((experts * capacity,), jnp.int32)
        .at[target]
        .set(jnp.arange(2 * row_count, dtype=jnp.int32) // 2)
    )
    outgoing = normed[source_row].reshape(experts, capacity, feat_width)
    w_gate = gate_proj[0]
    w_up = up_proj[0]
    w_down = down_proj[0]
    arrived_rows = lax.all_to_all(outgoing, "ep", split_axis=0, concat_axis=0, tiled=True)
    gate_part = jnp.einsum("scd,df->scf", arrived_rows, w_gate, preferred_element_type=jnp.float32)
    up_part = jnp.einsum("scd,df->scf", arrived_rows, w_up, preferred_element_type=jnp.float32)
    hidden = (jax.nn.silu(gate_part) * up_part).astype(jnp.bfloat16)
    expert_out = jnp.einsum(
        "scf,fd->scd",
        lax.all_gather(hidden, "tp", axis=2, tiled=True),
        w_down,
        preferred_element_type=jnp.float32,
    ).astype(jnp.bfloat16)
    returned = lax.all_to_all(expert_out, "ep", split_axis=0, concat_axis=0, tiled=True)
    picked = returned.reshape(experts * capacity, -1)[target].reshape(row_count, 2, -1)
    return jnp.sum(picked.astype(jnp.float32) * route_weights[:, :, None], axis=1).astype(
        jnp.bfloat16
    )


def on_device(
    queries,
    keys,
    values,
    gates,
    log_decay,
    out_weight,
    moe_rows,
    moe_gain,
    routes,
    route_weights,
    gate_proj,
    up_proj,
    down_proj,
):
    mixer_out = retention_half(queries, keys, values, gates, log_decay, out_weight)
    moe_out = expert_half(moe_rows, moe_gain, routes, route_weights, gate_proj, up_proj, down_proj)
    return (mixer_out, moe_out)


def solution(mesh):
    placed = (
        P("ep", "tp"),
        P("ep", "tp"),
        P("ep", "tp"),
        P("ep", "tp"),
        P("ep", "tp"),
        P(None, "tp"),
        P("ep", None),
        P(),
        P("ep", None),
        P("ep", None),
        P("ep", None, "tp"),
        P("ep", None, "tp"),
        P("ep", None, "tp"),
    )
    return jax.shard_map(
        on_device,
        mesh=mesh,
        in_specs=placed,
        out_specs=(P("ep", "tp"), P("ep", "tp")),
        check_vma=False,
    )
```

profile of v0, /device:TPU:0, one launch (start us, length us, event | category | flops | bytes accessed | tf_op | source)
XLA Modules:
  0.0 199.5 jit_solution(13536535929649242897)
XLA Ops:
  7.2 1.0 copy.86
  9.1 1.1 reduce-window.6
  10.9 2.4 %scatter_custom_fusion = s32[512]{0:T(512)S(1)} fusion(s32[512]{0:T(512)S(1)} %bitcast.110, s32[512]{0:T(512)S(1)} %add_select_fusion, s32[]{:T(128)} %copy.125), kind=kCustom, calls=%fused_computation.90 | custom fusion | bytes 2052 | tf_op jit(solution)/shard_map/scatter | solution.py:125
  13.4 0.7 convert_element_type.72
  14.1 1.5 fusion.9
  15.6 1.5 fusion.11
  17.2 3.3 %gather_fusion = bf16[512,2048]{1,0:T(8,128)(2,1)} fusion(bf16[256,2048]{1,0:T(8,128)(2,1)S(1)} %fusion.11, s32[1024]{0:T(1024)S(1)} %pad_clamp_fusion.1), kind=kCustom, calls=%fused_computation | custom fusion | bytes 4196352 | tf_op jit(solution)/shard_map/gather | solution.py:127
  20.5 6.5 %all-to-all-start = ((bf16[8,64,2048]{2,1,0:T(8,128)(2,1)}), bf16[8,64,2048]{2,1,0:T(8,128)(2,1)}, u32[]{:S(2)}, u32[]{:S(2)}) async-start(bf16[8,64,2048]{2,1,0:T(8,128)(2,1)} %bitcast.100), calls=%async_computation | async-start | bytes 4194304 | tf_op jit(solution)/shard_map/all_to_all | solution.py:131
  27.2 1.1 copy.93
  28.6 1.0 subtract_convert_fusion
  29.6 1.1 concatenate.20
  30.9 1.8 concatenate.21
  32.7 1.1 copy.73
  33.8 0.8 copy.91
  34.6 1.1 reduce_window_sum.37
  35.7 0.7 fusion.56
  36.5 1.0 copy.78
  37.5 1.7 reshape.218
  40.1 1.7 fusion.27
  41.8 1.7 while.29
  41.8 0.7 bitcast_dynamic-update-slice_fusion.3
  42.7 0.7 bitcast_dynamic-update-slice_fusion.3
  43.5 0.7 copy-done.1
  44.3 48.7 %all-to-all-done = bf16[8,64,2048]{2,1,0:T(8,128)(2,1)} async-done(((bf16[8,64,2048]{2,1,0:T(8,128)(2,1)}), bf16[8,64,2048]{2,1,0:T(8,128)(2,1)}, u32[]{:S(2)}, u32[]{:S(2)}) %all-to-all-start) | async-done | bytes 2097184 | tf_op jit(solution)/shard_map/all_to_all | solution.py:131
  92.9 5.3 %fusion.7 = f32[8,64,1024]{2,1,0:T(8,128)S(1)} fusion(bf16[8,64,2048]{2,1,0:T(8,128)(2,1)} %all-to-all-done, bf16[1,2048,1024]{2,1,0:T(8,128)(2,1)} %param.27), kind=kOutput, calls=%fused_computation.15 | convolution fusion | flops 2147483648 | bytes 8388608 | tf_op jit(solution)/shard_map/scd,df->scf/dot_general | solution.py:132
  98.3 5.2 %multiply_convert_fusion = bf16[8,64,1024]{2,1,0:T(8,128)(2,1)} fusion(f32[8,64,1024]{2,1,0:T(8,128)S(1)} %fusion.7, bf16[8,64,2048]{2,1,0:T(8,128)(2,1)} %all-to-all-done, bf16[1,2048,1024]{2,1,0:T(8,128)(2,1)S(1)} %copy-done.11), kind=kOutput, calls=%fused_computation.22 | convolution fusion | flops 2150629376 | bytes 9437184 | tf_op jit(solution)/shard_map/scd,df->scf/dot_general | solution.py:133
  105.0 14.7 %all-reduce = f32[32]{0:T(128)S(1)} all-reduce(f32[32]{0:T(128)S(1)} %exponential_dynamic-update-slice_fusion), channel_id=2, replica_groups=mesh['ep'=8,'tp'=4] {'ep'}, use_global_device_ids=true, to_apply=%add | all-reduce | flops 32 | bytes 256
  121.2 12.4 %while.30 = (s32[]{:T(128)}, f32[4,128,128]{2,1,0:T(8,128)S(1)}, s32[]{:T(128)}, f32[8,4]{1,0:T(8,128)}, f32[8,4,128,128]{3,2,1,0:T(8,128)}) while((s32[]{:T(128)}, f32[4,128,128]{2,1,0:T(8,128)S(1)}, s32[]{:T(128)}, f32[8,4]{1,0:T(8,128)}, f32[8,4,128,128]{3,2,1,0:T(8,128)}) %tuple.79), condition=%wide.region_6.7_spmd.clone.clone, body=%wide.region_5.6_spmd.clone.sunk.clone | while | flops 262148 | bytes 786569 | solution.py:20
  121.2 0.7 dynamic-slice_bitcast_fusion.3
  121.9 1.0 fusion.68
  123.7 1.0 fusion.68
  125.4 1.0 fusion.68
  127.2 1.0 fusion.68
  128.9 1.0 fusion.68
  130.7 1.1 fusion.68
  132.5 1.0 fusion.68
  133.6 2.5 %fusion.18 = f32[2,128,4,128]{1,3,2,0:T(8,128)} fusion(f32[2,4,128,128]{3,2,1,0:T(8,128)} %get-tuple-element.124, f32[2,128,4]{1,2,0:T(4,128)S(1)} %copy.82, f32[4,128,128]{2,1,0:T(8,128)S(1)} %get-tuple-element.126, f32[2,4]{1,0:T(2,128)S(1)} %subtract_exponential_fusion.1, bf16[2,128,4,64]{3,1,2,0:T(8,128)(2,1)S(1)} %copy.69, ...), kind=kOutput, calls=%fused_computation.28 | convolution fusion | flops 202244096 | bytes 1576992 | tf_op jit(solution)/shard_map/nihd,nhde->nihe/dot_general | solution.py:88
  136.1 2.4 %multiply_reduce_fusion.1 = (f32[2,128,4]{1,2,0:T(4,128)S(1)}, f32[2,128,4,128]{1,3,2,0:T(8,128)}) fusion(f32[2,128,4,128]{1,3,2,0:T(8,128)} %fusion.18, bf16[2,128,4,128]{3,2,1,0:T(4,128)(2,1)S(1)} %copy-done.4, bf16[2,128,4,128]{3,1,2,0:T(8,128)(2,1)S(1)} %copy-done.3, f32[2,4,128]{2,1,0:T(4,128)S(1)} %copy.75, ...), kind=kOutput, calls=%fused_computation.41 | convolution fusion | flops 68680704 | bytes 1859584 | tf_op jit(solution)/shard_map/nhij,njhd->nihd/dot_general | solution.py:69
  138.7 1.3 copy.83
  140.3 1.8 fusion.34
  142.2 13.0 %all-gather.8.cloned.1.call-done = bf16[8,64,4096]{2,1,0:T(8,128)(2,1)} async-done(((bf16[8,64,1024]{2,1,0:T(8,128)(2,1)}), bf16[8,64,4096]{2,1,0:T(8,128)(2,1)}) %all-gather.8.cloned.1.call-update) | async-done | bytes 4194320 | tf_op jit(solution)/shard_map/all_gather | solution.py:137
  155.2 6.6 %fusion.14 = bf16[8,64,512]{2,1,0:T(8,128)(2,1)} fusion(bf16[8,64,4096]{2,1,0:T(8,128)(2,1)} %all-gather.8.cloned.1.call-done, bf16[1,4096,512]{2,1,0:T(8,128)(2,1)} %param.29), kind=kOutput, calls=%fused_computation.23 | convolution fusion | flops 2147745792 | bytes 8912896 | tf_op jit(solution)/shard_map/scf,fd->scd/dot_general | solution.py:135
  161.8 4.6 %all-to-all-start.1 = ((bf16[8,64,512]{2,1,0:T(8,128)(2,1)}), bf16[8,64,512]{2,1,0:T(8,128)(2,1)S(1)}, u32[]{:S(2)}, u32[]{:S(2)}) async-start(bf16[8,64,512]{2,1,0:T(8,128)(2,1)} %fusion.14), calls=%async_computation.1 | async-start | bytes 1048576 | tf_op jit(solution)/shard_map/all_to_all | solution.py:141
  166.5 17.4 %all-gather.6.cloned.1.call-done = bf16[256,2048]{1,0:T(8,128)(2,1)} async-done(((bf16[256,512]{1,0:T(8,128)(2,1)}), bf16[256,2048]{1,0:T(8,128)(2,1)}) %all-gather.6.cloned.1.call-update) | async-done | bytes 1048592 | tf_op jit(solution)/shard_map/all_gather | solution.py:101
  184.0 2.6 %convolution_convert_fusion = bf16[256,512]{1,0:T(8,128)(2,1)} fusion(bf16[256,2048]{1,0:T(8,128)(2,1)} %all-gather.6.cloned.1.call-done, bf16[2048,512]{1,0:T(8,128)(2,1)S(1)} %copy-done), kind=kOutput, calls=%fused_computation.29 | convolution fusion | flops 537001984 | bytes 3407872 | tf_op jit(solution)/shard_map/dot_general | solution.py:100
  186.6 2.6 %gather_fusion.1 = bf16[512,512]{1,0:T(8,128)(2,1)} fusion(bf16[512,512]{1,0:T(8,128)(2,1)S(1)} %bitcast.99, s32[1024]{0:T(1024)S(1)} %pad_clamp_fusion), kind=kCustom, calls=%fused_computation.1 | custom fusion | bytes 1050624 | tf_op jit(solution)/shard_map/gather | solution.py:142
  189.2 1.7 reshape.227
  190.9 2.1 %multiply_reduce_fusion = bf16[256,512]{1,0:T(8,128)(2,1)} fusion(f32[256,2,512]{2,1,0:T(2,128)S(1)} %reshape.227, f32[256,2]{1,0:T(8,128)S(1)} %copy.88), kind=kLoop, calls=%fused_computation.31 | loop fusion | flops 393216 | bytes 1312768 | tf_op jit(solution)/shard_map/reduce_sum | solution.py:143
  (86 shorter events, 10.5 us)
Async XLA Ops:
  7.2 176.8 %copy-start = (bf16[2048,512]{1,0:T(8,128)(2,1)S(1)}, bf16[2048,512]{1,0:T(8,128)(2,1)}, u32[]{:S(2)}) copy-start(bf16[2048,512]{1,0:T(8,128)(2,1)} %param.22) | copy-start | bytes 6291460
  20.5 6.6 %copy-start.8 = (bf16[256,512]{1,0:T(8,128)(2,1)S(1)}, bf16[256,512]{1,0:T(8,128)(2,1)}, u32[]{:S(2)}) copy-start(bf16[256,512]{1,0:T(8,128)(2,1)} %param.17) | copy-start | bytes 786436
  20.5 72.5 %all-to-all-start = ((bf16[8,64,2048]{2,1,0:T(8,128)(2,1)}), bf16[8,64,2048]{2,1,0:T(8,128)(2,1)}, u32[]{:S(2)}, u32[]{:S(2)}) async-start(bf16[8,64,2048]{2,1,0:T(8,128)(2,1)} %bitcast.100), calls=%async_computation | async-start | bytes 4194304 | tf_op jit(solution)/shard_map/all_to_all | solution.py:131
  26.9 94.2 %all-gather.10.cloned.1.call-start = ((), (), s32[]{:S(2)}) async-start(), calls=%async_computation.4 | async-start | bytes 2359296 | tf_op jit(solution)/shard_map/all_gather | solution.py:11
  28.6 5.2 %copy-start.9 = (f32[256,4]{0,1:T(4,128)S(1)}, f32[256,4]{0,1:T(4,128)}, u32[]{:S(2)}) copy-start(f32[256,4]{0,1:T(4,128)} %param.21) | copy-start | bytes 12292
  39.4 0.7 copy-start.2
  43.5 0.7 copy-start.1
  44.2 110.9 %all-gather.8.cloned.1.call-start = ((), (), s32[]{:S(2)}) async-start(), calls=%async_computation.3 | async-start | bytes 5242880 | tf_op jit(solution)/shard_map/all_gather | solution.py:137
  92.9 5.3 %copy-start.11 = (bf16[1,2048,1024]{2,1,0:T(8,128)(2,1)S(1)}, bf16[1,2048,1024]{2,1,0:T(8,128)(2,1)}, u32[]{:S(2)}) copy-start(bf16[1,2048,1024]{2,1,0:T(8,128)(2,1)} %param.28) | copy-start | bytes 12582916
  98.2 5.4 %copy-start.12 = (u32[32]{0:T(128)S(1)}, u32[32]{0:T(128)}, u32[]{:S(2)}) copy-start(u32[32]{0:T(128)} %constant.105) | copy-start | bytes 388
  98.3 22.2 %copy-start.7 = (bf16[256,4,64]{0,2,1:T(8,128)(2,1)S(1)}, bf16[256,4,64]{0,2,1:T(8,128)(2,1)}, u32[]{:S(2)}) copy-start(bf16[256,4,64]{0,2,1:T(8,128)(2,1)} %get-tuple-element.183) | copy-start | bytes 393220
  98.3 22.4 %copy-start.6 = (bf16[256,4,64]{0,2,1:T(8,128)(2,1)S(1)}, bf16[256,4,64]{0,2,1:T(8,128)(2,1)}, u32[]{:S(2)}) copy-start(bf16[256,4,64]{0,2,1:T(8,128)(2,1)} %get-tuple-element.184) | copy-start | bytes 393220
  103.5 17.5 %copy-start.5 = (f32[2,128,4]{2,1,0:T(8,128)S(1)}, f32[2,128,4]{2,1,0:T(8,128)}, u32[]{:S(2)}) copy-start(f32[2,128,4]{2,1,0:T(8,128)} %get-tuple-element.191) | copy-start | bytes 12292
  103.5 80.5 %all-gather.6.cloned.1.call-start = ((), (), s32[]{:S(2)}) async-start(), calls=%async_computation.2 | async-start | bytes 1310720 | tf_op jit(solution)/shard_map/all_gather | solution.py:101
  121.2 14.9 %copy-start.3 = (bf16[2,128,4,128]{3,1,2,0:T(8,128)(2,1)S(1)}, bf16[2,128,4,128]{3,1,2,0:T(8,128)(2,1)}, u32[]{:S(2)}) copy-start(bf16[2,128,4,128]{3,1,2,0:T(8,128)(2,1)} %copy-done.2) | copy-start | bytes 786436
  121.2 14.9 %copy-start.4 = (bf16[2,128,4,128]{3,2,1,0:T(4,128)(2,1)S(1)}, bf16[2,128,4,128]{3,2,1,0:T(4,128)(2,1)}, u32[]{:S(2)}) copy-start(bf16[2,128,4,128]{3,2,1,0:T(4,128)(2,1)} %reshape.218) | copy-start | bytes 786436
  142.2 24.2 %copy-start.10 = (f32[256,2]{0,1:T(2,128)S(1)}, f32[256,2]{0,1:T(2,128)}, u32[]{:S(2)}) copy-start(f32[256,2]{0,1:T(2,128)} %param.26) | copy-start | bytes 6148
  161.8 24.8 %all-to-all-start.1 = ((bf16[8,64,512]{2,1,0:T(8,128)(2,1)}), bf16[8,64,512]{2,1,0:T(8,128)(2,1)S(1)}, u32[]{:S(2)}, u32[]{:S(2)}) async-start(bf16[8,64,512]{2,1,0:T(8,128)(2,1)} %fusion.14), calls=%async_computation.1 | async-start | bytes 1048576 | tf_op jit(solution)/shard_map/all_to_all | solution.py:141
Sparse Core Ops, SparseCore 0:
  44.3 48.1 all-gather.9
  103.6 51.5 all-gather.7
  157.6 26.3 all-gather.5
where the time goes:
time: 201 us; the launch traced here: 200 us
  waiting for transfers between devices  79.1 us (39%)
  local copies, waits for them, and re-layouts  30.9 us (15%)
  matrix products  26.4 us (13%)
  other arithmetic  22.1 us (11%)
  between operations  14.8 us (7%)
  blocking collectives  14.7 us (7%)
  starting transfers between devices  11.2 us (6%)
    all_to_all x1, waiting for transfers between devices, expert_half(): lax.all_to_all(outgoing, 'ep', split_axis=0, concat_axis=0, tiled=True)  48.7 us
    all_gather x1, waiting for transfers between devices, retention_half(): lax.all_gather(head_out, 'tp', axis=1, tiled=True)  17.4 us
    unnamed x1, blocking collectives  14.7 us
    all_gather x1, waiting for transfers between devices, expert_half(): lax.all_gather(hidden, 'tp', axis=2, tiled=True)  13 us
    select_n x7, other arithmetic, turn(): jnp.where(position < mine, new, old)  7.41 us
    dot_general x1, matrix products, expert_half(): jnp.einsum('scf,fd->scd', lax.all_gather(hidden, 'tp', axis=2, tiled=True...  6.6 us
    all_to_all x1, starting transfers between devices, expert_half(): lax.all_to_all(outgoing, 'ep', split_axis=0, concat_axis=0, tiled=True)  6.49 us
    dot_general x1, matrix products, expert_half(): jnp.einsum('scd,df->scf', arrived_rows, w_gate, preferred_element_type=jn...  5.3 us
  transfers between devices with their start and end apart: 5, of which 3 were waited for; matrix products, arithmetic and copies ran while one was open for 29% of the time, Pallas kernels for 0%

commit v1 on v0

--- a/solution.py
+++ b/solution.py
@@ -4,6 +4,22 @@
 from jax.sharding import PartitionSpec as P
 
 BLOCK = 128
+
+
+def ring_product(value, axis, dim, contribution):
+    peers, mine, span = (lax.axis_size(axis), lax.axis_index(axis), value.shape[dim])
+    forward = [(i, (i + 1) % peers) for i in range(peers)]
+    backward = [(i, (i - 1) % peers) for i in range(peers)]
+    halfway = peers // 2
+    from_left = from_right = value
+    subtotal = contribution(value, mine * span)
+    for step in range(1, halfway + 1):
+        from_left = lax.ppermute(from_left, axis, forward)
+        if step < peers - halfway:
+            from_right = lax.ppermute(from_right, axis, backward)
+            subtotal = subtotal + contribution(from_right, (mine + step) % peers * span)
+        subtotal = subtotal + contribution(from_left, (mine - step) % peers * span)
+    return subtotal
 
 
 def carried_in(value, axis, join, neutral):
@@ -132,11 +148,16 @@
     gate_part = jnp.einsum("scd,df->scf", arrived_rows, w_gate, preferred_element_type=jnp.float32)
     up_part = jnp.einsum("scd,df->scf", arrived_rows, w_up, preferred_element_type=jnp.float32)
     hidden = (jax.nn.silu(gate_part) * up_part).astype(jnp.bfloat16)
-    expert_out = jnp.einsum(
-        "scf,fd->scd",
-        lax.all_gather(hidden, "tp", axis=2, tiled=True),
-        w_down,
-        preferred_element_type=jnp.float32,
+    expert_out = ring_product(
+        hidden,
+        "tp",
+        2,
+        lambda shard, start: jnp.einsum(
+            "scf,fd->scd",
+            shard,
+            lax.dynamic_slice_in_dim(w_down, start, shard.shape[2], axis=0),
+            preferred_element_type=jnp.float32,
+        ),
     ).astype(jnp.bfloat16)
     returned = lax.all_to_all(expert_out, "ep", split_axis=0, concat_axis=0, tiled=True)
     picked = returned.reshape(experts * capacity, -1)[target].reshape(row_count, 2, -1)

time: 201 us -> 225 us (1.12)
  blocking collectives: 14.7 us -> 35.2 us
  waiting for transfers between devices: 79.1 us -> 64.9 us
  starting transfers between devices: 11.2 us -> 25.2 us
  matrix products: 26.4 us -> 29.1 us
    ppermute x0 -> x3, waiting for transfers between devices: none -> 41.7 us  [the longest x2 41.7 us: ring_product(): from_left = lax.ppermute(from_left, axis, forward)]
    all_to_all x1, waiting for transfers between devices: 48.7 us -> 10.6 us  [expert_half(): lax.all_to_all(outgoing, 'ep', split_axis=0, concat_axis=0, tiled=True)]
    unnamed x1, blocking collectives: 14.7 us -> 35.2 us
    all_gather x1, waiting for transfers between devices: 17.4 us -> 0.02 us  [retention_half(): lax.all_gather(head_out, 'tp', axis=1, tiled=True)]
    all_gather x1 -> x0, waiting for transfers between devices: 13 us -> none  [expert_half(): lax.all_gather(hidden, 'tp', axis=2, tiled=True)]
    all_to_all x1, waiting for transfers between devices: 0.01 us -> 12.5 us  [expert_half(): lax.all_to_all(expert_out, 'ep', split_axis=0, concat_axis=0, tiled=True)]
    all_to_all x1, starting transfers between devices: 4.61 us -> 14.7 us  [expert_half(): lax.all_to_all(expert_out, 'ep', split_axis=0, concat_axis=0, tiled=True)]
    ppermute x0 -> x3, starting transfers between devices: none -> 3.93 us  [the longest x1 2.44 us: ring_product(): from_right = lax.ppermute(from_right, axis, backward)]
  transfers between devices with their start and end apart: 5 -> 7, of which waited for: 3 -> 4; matrix products, arithmetic and copies ran while one was open for 29% -> 27% of each run, Pallas kernels for 0% -> 0%
where the time goes in v1:
time: 225 us; the launch traced here: 223 us
  waiting for transfers between devices  64.9 us (29%)
  blocking collectives  35.2 us (16%)
  local copies, waits for them, and re-layouts  31.4 us (14%)
  matrix products  29.1 us (13%)
  starting transfers between devices  25.2 us (11%)
  other arithmetic  22 us (10%)
  between operations  15.2 us (7%)
    ppermute x2, waiting for transfers between devices, ring_product(): from_left = lax.ppermute(from_left, axis, forward)  41.7 us
    unnamed x1, blocking collectives  35.2 us
    all_to_all x1, starting transfers between devices, expert_half(): lax.all_to_all(expert_out, 'ep', split_axis=0, concat_axis=0, tiled=True)  14.7 us
    all_to_all x1, waiting for transfers between devices, expert_half(): lax.all_to_all(expert_out, 'ep', split_axis=0, concat_axis=0, tiled=True)  12.5 us
    all_to_all x1, waiting for transfers between devices, expert_half(): lax.all_to_all(outgoing, 'ep', split_axis=0, concat_axis=0, tiled=True)  10.6 us
    dot_general x4, matrix products, expert_half(): jnp.einsum('scf,fd->scd', shard, lax.dynamic_slice_in_dim(w_down, start,...  9.31 us
    select_n x7, other arithmetic, turn(): jnp.where(position < mine, new, old)  7.34 us
    all_to_all x1, starting transfers between devices, expert_half(): lax.all_to_all(outgoing, 'ep', split_axis=0, concat_axis=0, tiled=True)  6.49 us
  transfers between devices with their start and end apart: 7, of which 4 were waited for; matrix products, arithmetic and copies ran while one was open for 27% of the time, Pallas kernels for 0%

profile of v1, /device:TPU:0, one launch (start us, length us, event | category | flops | bytes accessed | tf_op | source)
XLA Modules:
  0.0 223.3 jit_solution(7353413640624568495)
XLA Ops:
  7.2 1.0 copy.86
  9.1 1.1 reduce-window.6
  10.9 2.4 %scatter_custom_fusion = s32[512]{0:T(512)S(1)} fusion(s32[512]{0:T(512)S(1)} %bitcast.123, s32[512]{0:T(512)S(1)} %add_select_fusion, s32[]{:T(128)} %copy.125), kind=kCustom, calls=%fused_computation.100 | custom fusion | bytes 2052 | tf_op jit(solution)/shard_map/scatter | solution.py:141
  14.1 1.5 fusion.7
  15.6 1.5 fusion.9
  17.2 3.3 %gather_fusion = bf16[512,2048]{1,0:T(8,128)(2,1)} fusion(bf16[256,2048]{1,0:T(8,128)(2,1)S(1)} %fusion.9, s32[1024]{0:T(1024)S(1)} %pad_clamp_fusion.1), kind=kCustom, calls=%fused_computation | custom fusion | bytes 4196352 | tf_op jit(solution)/shard_map/gather | solution.py:143
  20.5 6.5 %all-to-all-start = ((bf16[8,64,2048]{2,1,0:T(8,128)(2,1)}), bf16[8,64,2048]{2,1,0:T(8,128)(2,1)}, u32[]{:S(2)}, u32[]{:S(2)}) async-start(bf16[8,64,2048]{2,1,0:T(8,128)(2,1)} %bitcast.113), calls=%async_computation | async-start | bytes 4194304 | tf_op jit(solution)/shard_map/all_to_all | solution.py:147
  27.2 1.1 copy.93
  28.6 1.0 subtract_convert_fusion
  29.6 1.1 concatenate.20
  30.9 1.8 concatenate.21
  32.7 1.1 copy.73
  33.8 0.8 copy.91
  34.6 1.1 reduce_window_sum.37
  36.5 1.0 copy.78
  37.5 1.7 reshape.222
  40.1 1.7 fusion.32
  41.9 1.7 while.29
  45.9 35.2 %all-reduce = f32[32]{0:T(128)S(1)} all-reduce(f32[32]{0:T(128)S(1)} %exponential_dynamic-update-slice_fusion), channel_id=2, replica_groups=mesh['ep'=8,'tp'=4] {'ep'}, use_global_device_ids=true, to_apply=%add | all-reduce | flops 32 | bytes 256
  82.5 10.6 %all-to-all-done = bf16[8,64,2048]{2,1,0:T(8,128)(2,1)} async-done(((bf16[8,64,2048]{2,1,0:T(8,128)(2,1)}), bf16[8,64,2048]{2,1,0:T(8,128)(2,1)}, u32[]{:S(2)}, u32[]{:S(2)}) %all-to-all-start) | async-done | bytes 2097184 | tf_op jit(solution)/shard_map/all_to_all | solution.py:147
  93.1 5.3 %fusion.5 = f32[8,64,1024]{2,1,0:T(8,128)S(1)} fusion(bf16[8,64,2048]{2,1,0:T(8,128)(2,1)} %all-to-all-done, bf16[1,2048,1024]{2,1,0:T(8,128)(2,1)} %param.27), kind=kOutput, calls=%fused_computation.13 | convolution fusion | flops 2147483648 | bytes 8388608 | tf_op jit(solution)/shard_map/scd,df->scf/dot_general | solution.py:148
  98.4 5.1 %multiply_convert_fusion = bf16[8,64,1024]{2,1,0:T(8,128)(2,1)} fusion(f32[8,64,1024]{2,1,0:T(8,128)S(1)} %fusion.5, bf16[8,64,2048]{2,1,0:T(8,128)(2,1)} %all-to-all-done, bf16[1,2048,1024]{2,1,0:T(8,128)(2,1)S(1)} %copy-done.12), kind=kOutput, calls=%fused_computation.20 | convolution fusion | flops 2150629376 | bytes 9437184 | tf_op jit(solution)/shard_map/scd,df->scf/dot_general | solution.py:149
  103.5 2.4 %collective-permute-start = (bf16[8,64,1024]{2,1,0:T(8,128)(2,1)}, bf16[8,64,1024]{2,1,0:T(8,128)(2,1)}, u32[]{:S(2)}, u32[]{:S(2)}) collective-permute-start(bf16[8,64,1024]{2,1,0:T(8,128)(2,1)} %multiply_convert_fusion), channel_id=1, source_target_pairs={{0,3},{1,0},{2,1},{3,2},{4,7},{5,4},{6,5},{7,6},{8,11},{9,8},{10,9... | collective-permute-start | bytes 3145736 | tf_op jit(solution)/shard_map/ppermute | solution.py:19
  106.0 12.4 %while.30 = (s32[]{:T(128)}, f32[4,128,128]{2,1,0:T(8,128)S(1)}, s32[]{:T(128)}, f32[8,4]{1,0:T(8,128)}, f32[8,4,128,128]{3,2,1,0:T(8,128)}) while((s32[]{:T(128)}, f32[4,128,128]{2,1,0:T(8,128)S(1)}, s32[]{:T(128)}, f32[8,4]{1,0:T(8,128)}, f32[8,4,128,128]{3,2,1,0:T(8,128)}) %tuple.77), condition=%wide.region_6.7_spmd.clone.clone, body=%wide.region_5.6_spmd.clone.sunk.clone | while | flops 262148 | bytes 786569 | solution.py:36
  106.8 1.0 fusion.80
  108.5 1.0 fusion.80
  110.3 1.0 fusion.80
  112.0 1.0 fusion.80
  113.8 1.0 fusion.80
  115.6 1.0 fusion.80
  117.3 1.0 fusion.80
  118.4 2.6 %fusion.14 = f32[2,128,4,128]{1,3,2,0:T(8,128)} fusion(f32[2,4,128,128]{3,2,1,0:T(8,128)} %get-tuple-element.124, f32[2,128,4]{1,2,0:T(4,128)S(1)} %copy.82, f32[4,128,128]{2,1,0:T(8,128)S(1)} %get-tuple-element.126, f32[2,4]{1,0:T(2,128)S(1)} %subtract_exponential_fusion.1, bf16[2,128,4,64]{3,1,2,0:T(8,128)(2,1)S(1)} %copy.69, ...), kind=kOutput, calls=%fused_computation.29 | convolution fusion | flops 202244096 | bytes 1576992 | tf_op jit(solution)/shard_map/nihd,nhde->nihe/dot_general | solution.py:104
  120.9 2.4 %multiply_reduce_fusion.1 = (f32[2,128,4]{1,2,0:T(4,128)S(1)}, f32[2,128,4,128]{1,3,2,0:T(8,128)}) fusion(f32[2,128,4,128]{1,3,2,0:T(8,128)} %fusion.14, bf16[2,128,4,128]{3,2,1,0:T(4,128)(2,1)S(1)} %copy-done.5, bf16[2,128,4,128]{3,1,2,0:T(8,128)(2,1)S(1)} %copy-done.4, f32[2,4,128]{2,1,0:T(4,128)S(1)} %copy.75, ...), kind=kOutput, calls=%fused_computation.51 | convolution fusion | flops 68680704 | bytes 1859584 | tf_op jit(solution)/shard_map/nhij,njhd->nihd/dot_general | solution.py:85
  123.6 1.3 copy.83
  124.8 24.9 %collective-permute-done.1 = bf16[8,64,1024]{2,1,0:T(8,128)(2,1)} collective-permute-done((bf16[8,64,1024]{2,1,0:T(8,128)(2,1)}, bf16[8,64,1024]{2,1,0:T(8,128)(2,1)}, u32[]{:S(2)}, u32[]{:S(2)}) %collective-permute-start.1) | collective-permute-done | bytes 1048608 | tf_op jit(solution)/shard_map/ppermute | solution.py:17
  149.7 1.5 collective-permute-start.2
  151.5 1.8 fusion.39
  153.4 2.3 %fusion.19 = f32[8,64,512]{2,1,0:T(8,128)S(1)} fusion(bf16[8,64,1024]{2,1,0:T(8,128)(2,1)} %multiply_convert_fusion, bf16[1,4096,512]{2,1,0:T(8,128)(2,1)} %param.29, s32[]{:T(128)S(6)} %select_n.80), kind=kOutput, calls=%fused_computation.35 | convolution fusion | flops 536870912 | bytes 3145732 | tf_op jit(solution)/shard_map/scf,fd->scd/dot_general | solution.py:155
  155.7 2.4 %convolution_add_fusion.2 = f32[8,64,512]{2,1,0:T(8,128)S(1)} fusion(f32[8,64,512]{2,1,0:T(8,128)S(1)} %fusion.19, bf16[8,64,1024]{2,1,0:T(8,128)(2,1)} %collective-permute-done, bf16[1,4096,512]{2,1,0:T(8,128)(2,1)} %param.29, s32[]{:T(128)S(6)} %select_n.82), kind=kOutput, calls=%fused_computation.23 | convolution fusion | flops 537133056 | bytes 4194308 | tf_op jit(solution)/shard_map/scf,fd->scd/dot_general | solution.py:155
  158.5 1.9 convolution_add_fusion.1
  160.4 16.9 %collective-permute-done.2 = bf16[8,64,1024]{2,1,0:T(8,128)(2,1)} collective-permute-done((bf16[8,64,1024]{2,1,0:T(8,128)(2,1)}, bf16[8,64,1024]{2,1,0:T(8,128)(2,1)}, u32[]{:S(2)}, u32[]{:S(2)}) %collective-permute-start.2) | collective-permute-done | bytes 1048608 | tf_op jit(solution)/shard_map/ppermute | solution.py:17
  177.3 2.7 %fusion.12 = bf16[8,64,512]{2,1,0:T(8,128)(2,1)} fusion(f32[8,64,512]{2,1,0:T(8,128)S(1)} %convolution_add_fusion.1, bf16[8,64,1024]{2,1,0:T(8,128)(2,1)} %collective-permute-done.2, bf16[1,4096,512]{2,1,0:T(8,128)(2,1)S(1)} %copy-done.2, s32[]{:T(128)S(6)} %select_n.86), kind=kOutput, calls=%fused_computation.24 | convolution fusion | flops 537395200 | bytes 3670020 | tf_op jit(solution)/shard_map/scf,fd->scd/dot_general | solution.py:155
  180.0 14.7 %all-to-all-start.1 = ((bf16[8,64,512]{2,1,0:T(8,128)(2,1)}), bf16[8,64,512]{2,1,0:T(8,128)(2,1)S(1)}, u32[]{:S(2)}, u32[]{:S(2)}) async-start(bf16[8,64,512]{2,1,0:T(8,128)(2,1)} %fusion.12), calls=%async_computation.1 | async-start | bytes 1048576 | tf_op jit(solution)/shard_map/all_to_all | solution.py:162
  194.9 2.6 %convolution_convert_fusion = bf16[256,512]{1,0:T(8,128)(2,1)} fusion(bf16[256,2048]{1,0:T(8,128)(2,1)} %all-gather.5.cloned.1.call-done, bf16[2048,512]{1,0:T(8,128)(2,1)S(1)} %copy-done), kind=kOutput, calls=%fused_computation.30 | convolution fusion | flops 537001984 | bytes 3407872 | tf_op jit(solution)/shard_map/dot_general | solution.py:116
  197.6 12.5 %all-to-all-done.1 = bf16[8,64,512]{2,1,0:T(8,128)(2,1)S(1)} async-done(((bf16[8,64,512]{2,1,0:T(8,128)(2,1)}), bf16[8,64,512]{2,1,0:T(8,128)(2,1)S(1)}, u32[]{:S(2)}, u32[]{:S(2)}) %all-to-all-start.1) | async-done | bytes 524320 | tf_op jit(solution)/shard_map/all_to_all | solution.py:162
  210.1 2.6 %gather_fusion.1 = bf16[512,512]{1,0:T(8,128)(2,1)} fusion(bf16[512,512]{1,0:T(8,128)(2,1)S(1)} %bitcast.112, s32[1024]{0:T(1024)S(1)} %pad_clamp_fusion), kind=kCustom, calls=%fused_computation.1 | custom fusion | bytes 1050624 | tf_op jit(solution)/shard_map/gather | solution.py:163
  212.7 1.7 reshape.231
  214.4 2.1 multiply_reduce_fusion
  (94 shorter events, 15.2 us)
Async XLA Ops:
  7.2 187.8 %copy-start = (bf16[2048,512]{1,0:T(8,128)(2,1)S(1)}, bf16[2048,512]{1,0:T(8,128)(2,1)}, u32[]{:S(2)}) copy-start(bf16[2048,512]{1,0:T(8,128)(2,1)} %param.22) | copy-start | bytes 6291460
  20.5 6.6 %copy-start.9 = (bf16[256,512]{1,0:T(8,128)(2,1)S(1)}, bf16[256,512]{1,0:T(8,128)(2,1)}, u32[]{:S(2)}) copy-start(bf16[256,512]{1,0:T(8,128)(2,1)} %param.17) | copy-start | bytes 786436
  20.5 72.7 %all-to-all-start = ((bf16[8,64,2048]{2,1,0:T(8,128)(2,1)}), bf16[8,64,2048]{2,1,0:T(8,128)(2,1)}, u32[]{:S(2)}, u32[]{:S(2)}) async-start(bf16[8,64,2048]{2,1,0:T(8,128)(2,1)} %bitcast.113), calls=%async_computation | async-start | bytes 4194304 | tf_op jit(solution)/shard_map/all_to_all | solution.py:147
  26.9 79.1 %all-gather.7.cloned.1.call-start = ((), (), s32[]{:S(2)}) async-start(), calls=%async_computation.3 | async-start | bytes 2359296 | tf_op jit(solution)/shard_map/all_gather | solution.py:27
  28.6 5.2 %copy-start.10 = (f32[256,4]{0,1:T(4,128)S(1)}, f32[256,4]{0,1:T(4,128)}, u32[]{:S(2)}) copy-start(f32[256,4]{0,1:T(4,128)} %param.21) | copy-start | bytes 12292
  39.4 0.7 copy-start.3
  41.8 2.6 %copy-start.13 = (u32[32]{0:T(128)S(1)}, u32[32]{0:T(128)}, u32[]{:S(2)}) copy-start(u32[32]{0:T(128)} %constant.140) | copy-start | bytes 388
  41.8 40.0 %copy-start.8 = (bf16[256,4,64]{0,2,1:T(8,128)(2,1)S(1)}, bf16[256,4,64]{0,2,1:T(8,128)(2,1)}, u32[]{:S(2)}) copy-start(bf16[256,4,64]{0,2,1:T(8,128)(2,1)} %get-tuple-element.183) | copy-start | bytes 393220
  41.8 40.2 %copy-start.7 = (bf16[256,4,64]{0,2,1:T(8,128)(2,1)S(1)}, bf16[256,4,64]{0,2,1:T(8,128)(2,1)}, u32[]{:S(2)}) copy-start(bf16[256,4,64]{0,2,1:T(8,128)(2,1)} %get-tuple-element.184) | copy-start | bytes 393220
  41.9 40.5 %copy-start.6 = (f32[2,128,4]{2,1,0:T(8,128)S(1)}, f32[2,128,4]{2,1,0:T(8,128)}, u32[]{:S(2)}) copy-start(f32[2,128,4]{2,1,0:T(8,128)} %get-tuple-element.191) | copy-start | bytes 12292
  43.6 0.7 copy-start.1
  44.3 150.6 %all-gather.5.cloned.1.call-start = ((), (), s32[]{:S(2)}) async-start(), calls=%async_computation.2 | async-start | bytes 1310720 | tf_op jit(solution)/shard_map/all_gather | solution.py:117
  93.1 5.3 %copy-start.12 = (bf16[1,2048,1024]{2,1,0:T(8,128)(2,1)S(1)}, bf16[1,2048,1024]{2,1,0:T(8,128)(2,1)}, u32[]{:S(2)}) copy-start(bf16[1,2048,1024]{2,1,0:T(8,128)(2,1)} %param.28) | copy-start | bytes 12582916
  103.5 52.1 %collective-permute-start = (bf16[8,64,1024]{2,1,0:T(8,128)(2,1)}, bf16[8,64,1024]{2,1,0:T(8,128)(2,1)}, u32[]{:S(2)}, u32[]{:S(2)}) collective-permute-start(bf16[8,64,1024]{2,1,0:T(8,128)(2,1)} %multiply_convert_fusion), channel_id=1, source_target_pairs={{0,3},{1,0},{2,1},{3,2},{4,7},{5,4},{6,5},{7,6},{8,11},{9,8},{10,9... | collective-permute-start | bytes 3145736 | tf_op jit(solution)/shard_map/ppermute | solution.py:19
  106.0 43.7 %collective-permute-start.1 = (bf16[8,64,1024]{2,1,0:T(8,128)(2,1)}, bf16[8,64,1024]{2,1,0:T(8,128)(2,1)}, u32[]{:S(2)}, u32[]{:S(2)}) collective-permute-start(bf16[8,64,1024]{2,1,0:T(8,128)(2,1)} %multiply_convert_fusion), channel_id=1, source_target_pairs={{0,1},{1,2},{2,3},{3,0},{4,5},{5,6},{6,7},{7,4},{8,9},{9,10},{10,1... | collective-permute-start | bytes 3145736 | tf_op jit(solution)/shard_map/ppermute | solution.py:17
  106.0 14.9 %copy-start.4 = (bf16[2,128,4,128]{3,1,2,0:T(8,128)(2,1)S(1)}, bf16[2,128,4,128]{3,1,2,0:T(8,128)(2,1)}, u32[]{:S(2)}) copy-start(bf16[2,128,4,128]{3,1,2,0:T(8,128)(2,1)} %copy-done.3) | copy-start | bytes 786436
  106.0 14.9 %copy-start.5 = (bf16[2,128,4,128]{3,2,1,0:T(4,128)(2,1)S(1)}, bf16[2,128,4,128]{3,2,1,0:T(4,128)(2,1)}, u32[]{:S(2)}) copy-start(bf16[2,128,4,128]{3,2,1,0:T(4,128)(2,1)} %reshape.222) | copy-start | bytes 786436
  149.7 27.6 %collective-permute-start.2 = (bf16[8,64,1024]{2,1,0:T(8,128)(2,1)}, bf16[8,64,1024]{2,1,0:T(8,128)(2,1)}, u32[]{:S(2)}, u32[]{:S(2)}) collective-permute-start(bf16[8,64,1024]{2,1,0:T(8,128)(2,1)} %collective-permute-done.1), channel_id=1, source_target_pairs={{0,1},{1,2},{2,3},{3,0},{4,5},{5,6},{6,7},{7,4},{8,9},{9,10},{10,1... | collective-permute-start | bytes 3145736 | tf_op jit(solution)/shard_map/ppermute | solution.py:17
  155.6 2.8 %copy-start.2 = (bf16[1,4096,512]{2,1,0:T(8,128)(2,1)S(1)}, bf16[1,4096,512]{2,1,0:T(8,128)(2,1)}, u32[]{:S(2)}) copy-start(bf16[1,4096,512]{2,1,0:T(8,128)(2,1)} %param.29) | copy-start | bytes 12582916
  160.4 34.3 %copy-start.11 = (f32[256,2]{0,1:T(2,128)S(1)}, f32[256,2]{0,1:T(2,128)}, u32[]{:S(2)}) copy-start(f32[256,2]{0,1:T(2,128)} %param.26) | copy-start | bytes 6148
  180.0 30.1 %all-to-all-start.1 = ((bf16[8,64,512]{2,1,0:T(8,128)(2,1)}), bf16[8,64,512]{2,1,0:T(8,128)(2,1)S(1)}, u32[]{:S(2)}, u32[]{:S(2)}) async-start(bf16[8,64,512]{2,1,0:T(8,128)(2,1)} %fusion.12), calls=%async_computation.1 | async-start | bytes 1048576 | tf_op jit(solution)/shard_map/all_to_all | solution.py:162
Sparse Core Ops, SparseCore 0:
  44.4 48.2 all-gather.6
  153.5 35.6 all-gather.4
